TPU v7x, 256 devices: a 4x2x16 block of a 4x16x16 slice. The times are simulated.
256 devices in a mesh: grp: 2 (over y), fs: 16 (over z), tp: 8 (over x, core).
Axes of the slice: x: 4, y: 2, z: 16, core: 2. Of those that a mesh axis runs over, the one named last changes fastest.
The devices are a block of a 4x16x16 slice.
Arguments:
- tokens: bfloat16 [32768, 2048], P(('grp', 'fs', 'tp')), parts along dimension 0, may hold values from -12 to 12
- norm_gain: float32 [2048], replicated, may hold values from 0.1 to 1.9
- w_in: bfloat16 [2048, 8192], P('fs', 'tp'), may hold values from -0.125 to 0.125
- w_out: bfloat16 [8192, 2048], P('tp', 'fs'), may hold values from -0.0625 to 0.0625
Outputs:
- mixed: bfloat16 [32768, 2048], P(('grp', 'fs', 'tp')), parts along dimension 0
There are 2 independent parts, one for each index of `grp`. A program takes and returns all parts, laid end to end along the dimension named above; an argument that names none is the same for every part. Nothing has to cross between parts.
All inputs are finite; a program needn't handle non-finite values.
Results may differ from a plain program's by a relative error of at most 0.012.
Values may be sent and summed in bfloat16 or wider, within the bound.
No kernel may reach another device: no remote copies, remote signals or barrier semaphores. Data moves between devices by JAX's collectives and lax.ppermute only.
A program may use at most 64 MiB of HBM per device.

v0:
```python
import jax
import jax.numpy as jnp
from jax import lax
from jax.sharding import PartitionSpec as P

EPS = 1e-06


def from_everyone(shard, axis):
    copies = jnp.broadcast_to(shard, (lax.axis_size(axis), *shard.shape))
    return lax.all_to_all(copies, axis, split_axis=0, concat_axis=0, tiled=True)


def joined_along(parts, dim):
    parts = jnp.moveaxis(parts, 0, dim)
    shape = parts.shape
    return parts.reshape(*shape[:dim], shape[dim] * shape[dim + 1], *shape[dim + 2 :])


def collect(shard, axis, dim):
    parts = from_everyone(shard, axis)
    return joined_along(parts, dim)


def local(tokens, norm_gain, w_in, w_out):
    xf = tokens.astype(jnp.float32)
    scale = lax.rsqrt(jnp.mean(xf * xf, axis=-1, keepdims=True) + EPS)
    normed = (xf * scale * norm_gain).astype(jnp.bfloat16)
    whole_in = lax.all_gather(w_in, "fs", axis=0, tiled=True)
    pre = jnp.dot(collect(normed, "tp", 0), whole_in, preferred_element_type=jnp.float32)
    hidden = jnp.square(jax.nn.relu(pre)).astype(jnp.bfloat16)
    whole_out = lax.all_gather(w_out, "fs", axis=1, tiled=True)
    summed = lax.psum_scatter(
        jnp.dot(hidden, whole_out, preferred_element_type=jnp.float32).astype(jnp.bfloat16),
        "tp",
        scatter_dimension=0,
        tiled=True,
    ).astype(jnp.float32)
    return (xf + summed).astype(jnp.bfloat16)


def solution(mesh):
    in_specs = (P(("grp", "fs", "tp"), None), P(), P("fs", "tp"), P("tp", "fs"))
    out_specs = P(("grp", "fs", "tp"), None)
    return jax.shard_map(local, mesh=mesh, in_specs=in_specs, out_specs=out_specs, check_vma=False)
```

profile of v0, /device:TPU:40, one launch (start us, length us, event | category | flops | bytes accessed | tf_op | source)
XLA Modules:
  0.0 253.1 jit_solution(16195759570042781914)
XLA Ops:
  6.5 0.0 all-gather.3.cloned.1.call-start
  6.6 0.7 all-gather.3.cloned.1.call-update
  7.3 0.1 all-gather.5.cloned.1.call-start
  7.4 0.7 all-gather.5.cloned.1.call-update
  8.1 0.1 reduce-scatter.2.cloned.1.call-start
  8.2 1.2 fusion
  9.4 1.2 fusion.2
  10.7 0.5 broadcast_in_dim.2
  11.2 54.2 %all_to_all.5 = bf16[8,128,2048]{2,1,0:T(8,128)(2,1)} all-to-all(bf16[8,128,2048]{2,1,0:T(8,128)(2,1)S(1)} %broadcast_in_dim.2), channel_id=1, replica_groups=mesh['grp'=2,'fs'=16,'tp'=8] {'tp'}, dimensions={0} | all-to-all | bytes 8388608 | tf_op jit(solution)/shard_map/all_to_all | solution.py:11
  65.4 33.0 %all-gather.3.cloned.1.call-done = bf16[2048,1024]{1,0:T(8,128)(2,1)} async-done(((bf16[128,1024]{1,0:T(8,128)(2,1)}), bf16[2048,1024]{1,0:T(8,128)(2,1)}) %all-gather.3.cloned.1.call-update) | async-done | bytes 4194320 | tf_op jit(solution)/shard_map/all_gather | solution.py:29
  98.3 91.3 %all-gather.5.cloned.1.call-done = bf16[1024,2048]{1,0:T(8,128)(2,1)} async-done(((bf16[1024,128]{1,0:T(8,128)(2,1)}), bf16[1024,2048]{1,0:T(8,128)(2,1)}) %all-gather.5.cloned.1.call-update) | async-done | bytes 4194320 | tf_op jit(solution)/shard_map/all_gather | solution.py:32
  189.6 14.4 %convolution_convert_fusion = bf16[1024,2048]{1,0:T(8,128)(2,1)} fusion(bf16[1024,2048]{1,0:T(8,128)(2,1)} %all-gather.5.cloned.1.call-done, bf16[1024,2048]{1,0:T(8,128)(2,1)} %bitcast.4, bf16[2048,1024]{1,0:T(8,128)(2,1)} %all-gather.3.cloned.1.call-done), kind=kOutput, calls=%fused_computation.1 | convolution fusion | flops 8595177472 | bytes 16777216 | tf_op jit(solution)/shard_map/dot_general | solution.py:34
  204.0 0.0 copy-start
  204.0 0.1 reduce-scatter.2.cloned.1.call-update
  204.1 40.5 %reduce-scatter.2.cloned.1.call-done = bf16[128,2048]{1,0:T(8,128)(2,1)} async-done(((bf16[1024,2048]{1,0:T(8,128)(2,1)}), bf16[128,2048]{1,0:T(8,128)(2,1)}) %reduce-scatter.2.cloned.1.call-update) | async-done | bytes 524304 | tf_op jit(solution)/shard_map/reduce_scatter | solution.py:33
  244.5 0.0 copy-done
  244.5 2.0 fusion.3
  (1 shorter events, 0.0 us)
Async XLA Ops:
  6.5 91.8 %all-gather.3.cloned.1.call-start = ((), (), s32[]{:S(2)}) async-start(), calls=%async_computation.2 | async-start | bytes 4456448 | tf_op jit(solution)/shard_map/all_gather | solution.py:29
  7.3 182.3 %all-gather.5.cloned.1.call-start = ((), (), s32[]{:S(2)}) async-start(), calls=%async_computation.3 | async-start | bytes 4456448 | tf_op jit(solution)/shard_map/all_gather | solution.py:32
  8.1 236.4 %reduce-scatter.2.cloned.1.call-start = ((), (), s32[]{:S(2)}) async-start(), calls=%async_computation.4 | async-start | bytes 4718592 | tf_op jit(solution)/shard_map/reduce_scatter | solution.py:33
  204.0 40.6 %copy-start = (bf16[128,2048]{1,0:T(8,128)(2,1)S(1)}, bf16[128,2048]{1,0:T(8,128)(2,1)}, u32[]{:S(2)}) copy-start(bf16[128,2048]{1,0:T(8,128)(2,1)} %param.4) | copy-start | bytes 1572868
Sparse Core Ops, SparseCore 0:
  9.1 89.1 all-gather.2
  100.1 89.5 all-gather.4
  204.2 40.3 reduce-scatter.1
where the time goes:
time: 253 us
  waiting for transfers between devices  166 us (66%)
  blocking collectives  54.2 us (21%)
  matrix products  14.4 us (6%)
  between operations  13.1 us (5%)
  other arithmetic  4.44 us (2%)
    all_gather x1, waiting for transfers between devices, local(): whole_out = lax.all_gather(w_out, 'fs', axis=1, tiled=True)  91.3 us
    all_to_all x1, blocking collectives, from_everyone(): return lax.all_to_all(copies, axis, split_axis=0, concat_axis=0, tiled=True)  54.2 us
    reduce_scatter x1, waiting for transfers between devices, local(): lax.psum_scatter(jnp.dot(hidden, whole_out, preferred_element_type=jnp.fl...  40.5 us
    all_gather x1, waiting for transfers between devices, local(): whole_in = lax.all_gather(w_in, 'fs', axis=0, tiled=True)  33 us
    dot_general x1, matrix products, local(): jnp.dot(hidden, whole_out, preferred_element_type=jnp.float32)  14.4 us
  transfers between devices with their start and end apart: 3, of which 3 were waited for; matrix products, arithmetic and copies ran while one was open for 1% of the time, Pallas kernels for 0%

commit v1 on v0

--- a/solution.py
+++ b/solution.py
@@ -29,7 +29,7 @@
     whole_in = lax.all_gather(w_in, "fs", axis=0, tiled=True)
     pre = jnp.dot(collect(normed, "tp", 0), whole_in, preferred_element_type=jnp.float32)
     hidden = jnp.square(jax.nn.relu(pre)).astype(jnp.bfloat16)
-    whole_out = lax.all_gather(w_out, "fs", axis=1, tiled=True)
+    whole_out = jnp.concatenate(lax.all_gather(w_out, "fs"), axis=1)
     summed = lax.psum_scatter(
         jnp.dot(hidden, whole_out, preferred_element_type=jnp.float32).astype(jnp.bfloat16),
         "tp",

time: 253 us -> 238 us (0.941)
  blocking collectives: 54.2 us -> 0 us
  waiting for transfers between devices: 166 us -> 192 us
  local copies, waits for them, and re-layouts: 0.52 us -> 8.84 us
  starting transfers between devices: 0.13 us -> 4.87 us
    all_to_all x1 -> x0, blocking collectives: 54.2 us -> none  [from_everyone(): return lax.all_to_all(copies, axis, split_axis=0, concat_axis=0, tiled=True)]
    all_gather x1, waiting for transfers between devices: 33 us -> 68.8 us  [local(): whole_in = lax.all_gather(w_in, 'fs', axis=0, tiled=True)]
    all_gather x1, waiting for transfers between devices: 91.3 us -> 80.5 us  [local(): whole_out = jnp.concatenate(lax.all_gather(w_out, 'fs'), axis=1)]
    reshape x0 -> x1, local copies, waits for them, and re-layouts: none -> 6.37 us  [local(): whole_out = jnp.concatenate(lax.all_gather(w_out, 'fs'), axis=1)]
    all_to_all x0 -> x1, starting transfers between devices: none -> 4.74 us  [from_everyone(): return lax.all_to_all(copies, axis, split_axis=0, concat_axis=0, tiled=True)]
  transfers between devices with their start and end apart: 3 -> 4, of which waited for: 3 -> 3; matrix products, arithmetic and copies ran while one was open for 1% -> 5% of each run, Pallas kernels for 0% -> 0%
where the time goes in v1:
time: 238 us; the launch traced here: 237 us
  waiting for transfers between devices  192 us (81%)
  matrix products  14.4 us (6%)
  between operations  13.1 us (6%)
  local copies, waits for them, and re-layouts  8.84 us (4%)
  starting transfers between devices  4.87 us (2%)
  other arithmetic  4.44 us (2%)
    all_gather x1, waiting for transfers between devices, local(): whole_out = jnp.concatenate(lax.all_gather(w_out, 'fs'), axis=1)  80.5 us
    all_gather x1, waiting for transfers between devices, local(): whole_in = lax.all_gather(w_in, 'fs', axis=0, tiled=True)  68.8 us
    reduce_scatter x1, waiting for transfers between devices, local(): lax.psum_scatter(jnp.dot(hidden, whole_out, preferred_element_type=jnp.fl...  40.8 us
    dot_general x1, matrix products, local(): jnp.dot(hidden, whole_out, preferred_element_type=jnp.float32)  14.4 us
    reshape x1, local copies, waits for them, and re-layouts, local(): whole_out = jnp.concatenate(lax.all_gather(w_out, 'fs'), axis=1)  6.37 us
  transfers between devices with their start and end apart: 4, of which 3 were waited for; matrix products, arithmetic and copies ran while one was open for 5% of the time, Pallas kernels for 0%

profile of v1, /device:TPU:40, one launch (start us, length us, event | category | flops | bytes accessed | tf_op | source)
XLA Modules:
  0.0 237.3 jit_solution(15323015785512215709)
XLA Ops:
  6.5 0.0 all-gather.6.cloned.1.call-start
  6.6 0.7 all-gather.6.cloned.1.call-update
  7.3 0.1 all-gather.4.cloned.1.call-start
  7.4 0.7 all-gather.4.cloned.1.call-update
  8.1 1.2 fusion
  9.4 1.2 fusion.2
  10.6 2.5 %broadcast_in_dim.2 = bf16[8,128,2048]{2,1,0:T(8,128)(2,1)} broadcast(bf16[128,2048]{1,0:T(8,128)(2,1)S(1)} %fusion.2), dimensions={1,2} | broadcast | bytes 4718592 | tf_op jit(solution)/shard_map/broadcast_in_dim | solution.py:10
  13.1 4.7 %all-to-all-start = ((bf16[8,128,2048]{2,1,0:T(8,128)(2,1)}), bf16[8,128,2048]{2,1,0:T(8,128)(2,1)}, u32[]{:S(2)}, u32[]{:S(2)}) async-start(bf16[8,128,2048]{2,1,0:T(8,128)(2,1)} %broadcast_in_dim.2), calls=%async_computation | async-start | bytes 8388608 | tf_op jit(solution)/shard_map/all_to_all | solution.py:11
  17.8 0.1 reduce-scatter.2.cloned.1.call-start
  17.9 80.5 %all-gather.6.cloned.1.call-done = bf16[16384,128]{1,0:T(8,128)(2,1)} async-done(((bf16[1024,128]{1,0:T(8,128)(2,1)}), bf16[16384,128]{1,0:T(8,128)(2,1)}) %all-gather.6.cloned.1.call-update) | async-done | bytes 4194320 | tf_op jit(solution)/shard_map/all_gather | solution.py:32
  98.3 6.4 %copy.5 = bf16[1024,16,128]{0,2,1:T(8,128)(2,1)} copy(bf16[1024,16,128]{2,0,1:T(8,128)(2,1)} %bitcast.8) | data formatting | bytes 8388608 | tf_op jit(solution)/shard_map/reshape | solution.py:32
  104.7 0.0 all-to-all-done
  104.7 68.8 %all-gather.4.cloned.1.call-done = bf16[2048,1024]{1,0:T(8,128)(2,1)} async-done(((bf16[128,1024]{1,0:T(8,128)(2,1)}), bf16[2048,1024]{1,0:T(8,128)(2,1)}) %all-gather.4.cloned.1.call-update) | async-done | bytes 4194320 | tf_op jit(solution)/shard_map/all_gather | solution.py:29
  173.5 14.4 %convolution_convert_fusion = bf16[1024,2048]{1,0:T(8,128)(2,1)} fusion(bf16[1024,2048]{0,1:T(8,128)(2,1)} %bitcast.9, bf16[1024,2048]{1,0:T(8,128)(2,1)} %bitcast, bf16[2048,1024]{1,0:T(8,128)(2,1)} %all-gather.4.cloned.1.call-done), kind=kOutput, calls=%fused_computation.1 | convolution fusion | flops 8595177472 | bytes 16777216 | tf_op jit(solution)/shard_map/dot_general | solution.py:34
  187.9 0.0 copy-start
  187.9 0.1 reduce-scatter.2.cloned.1.call-update
  188.0 40.8 %reduce-scatter.2.cloned.1.call-done = bf16[128,2048]{1,0:T(8,128)(2,1)} async-done(((bf16[1024,2048]{1,0:T(8,128)(2,1)}), bf16[128,2048]{1,0:T(8,128)(2,1)}) %reduce-scatter.2.cloned.1.call-update) | async-done | bytes 524304 | tf_op jit(solution)/shard_map/reduce_scatter | solution.py:33
  228.8 0.0 copy-done
  228.8 2.0 fusion.3
  (1 shorter events, 0.0 us)
Async XLA Ops:
  6.5 91.8 %all-gather.6.cloned.1.call-start = ((), (), s32[]{:S(2)}) async-start(), calls=%async_computation.4 | async-start | bytes 4456448 | tf_op jit(solution)/shard_map/all_gather | solution.py:32
  7.3 166.2 %all-gather.4.cloned.1.call-start = ((), (), s32[]{:S(2)}) async-start(), calls=%async_computation.2 | async-start | bytes 4456448 | tf_op jit(solution)/shard_map/all_gather | solution.py:29
  13.1 91.7 %all-to-all-start = ((bf16[8,128,2048]{2,1,0:T(8,128)(2,1)}), bf16[8,128,2048]{2,1,0:T(8,128)(2,1)}, u32[]{:S(2)}, u32[]{:S(2)}) async-start(bf16[8,128,2048]{2,1,0:T(8,128)(2,1)} %broadcast_in_dim.2), calls=%async_computation | async-start | bytes 8388608 | tf_op jit(solution)/shard_map/all_to_all | solution.py:11
  17.8 210.9 %reduce-scatter.2.cloned.1.call-start = ((), (), s32[]{:S(2)}) async-start(), calls=%async_computation.3 | async-start | bytes 4718592 | tf_op jit(solution)/shard_map/reduce_scatter | solution.py:33
  187.9 40.9 %copy-start = (bf16[128,2048]{1,0:T(8,128)(2,1)S(1)}, bf16[128,2048]{1,0:T(8,128)(2,1)}, u32[]{:S(2)}) copy-start(bf16[128,2048]{1,0:T(8,128)(2,1)} %param.4) | copy-start | bytes 1572868
Sparse Core Ops, SparseCore 0:
  9.1 89.1 all-gather.5
  100.1 73.3 all-gather.3
  188.1 40.6 reduce-scatter.1
